TPU v7x, 256 devices: a whole 4x4x8 slice. The times are simulated.
256 devices in a mesh: ep: 64 (over z, x, core), tp: 4 (over y).
Axes of the slice: x: 4, y: 4, z: 8, core: 2. Of those that a mesh axis runs over, the one named last changes fastest.
Arguments:
- mix_input: bfloat16 [65536, 1024], P(('ep', 'tp')), may hold values from -6 to 6
- pool_weight: bfloat16 [8, 128, 128], replicated, may hold values from -0.5 to 0.5
- pool_scale: float32 [1024], replicated, may hold values from 0.1 to 1.9
- out_weight: bfloat16 [1024, 2048], replicated, may hold values from -0.1875 to 0.1875
- moe_input: bfloat16 [8192, 2048], P('ep'), may hold values from -6 to 6
- moe_gain: float32 [2048], replicated, may hold values from 0.1 to 1.9
- group_router: bfloat16 [2048, 4], replicated, may hold values from -0.125 to 0.125
- inner_router: bfloat16 [2048, 64], replicated, may hold values from -0.125 to 0.125
- group_pick: int32 [8192], P('ep'), may hold values from 0 to 3
- inner_pick: int32 [8192, 2], P('ep'), may hold values from 0 to 15, all different within a row
- gate_weight: bfloat16 [64, 2048, 1024], P('ep', None, 'tp'), may hold values from -0.125 to 0.125
- up_weight: bfloat16 [64, 2048, 1024], P('ep', None, 'tp'), may hold values from -0.125 to 0.125
- down_weight: bfloat16 [64, 1024, 2048], P('ep', 'tp'), may hold values from -0.1875 to 0.1875
Outputs:
- mix_out: bfloat16 [65536, 2048], P(('ep', 'tp'))
- moe_out: bfloat16 [8192, 2048], P('ep', 'tp')
All inputs are finite; a program needn't handle non-finite values.
Results may differ from a plain program's by a relative error of at most 0.011.
Values may be sent and summed in bfloat16 or wider, within the bound.
A program may use at most 64 MiB of HBM per device.

v0:
```python
import jax
import jax.numpy as jnp
from jax import lax
from jax.sharding import PartitionSpec as P

WINDOW_MAX = 16


NORM_FLOOR = 0.25


def passed_along(value, axis, steps):
    count = lax.axis_size(axis)
    first, last = (max(0, -steps), min(count, count - steps))
    return lax.ppermute(value, axis, [(source, source + steps) for source in range(first, last)])


def in_order(blocks, dim):
    lengths = list(blocks.shape[1:])
    lengths[dim] *= blocks.shape[0]
    return jnp.moveaxis(blocks, 0, dim).reshape(lengths)


def sent_to_all(array, axis):
    count = lax.axis_size(axis)
    return lax.all_to_all(
        jnp.broadcast_to(array[None], (count, *array.shape)), axis, 0, 0, tiled=True
    )


def gather_directly(array, axis, dim):
    return in_order(sent_to_all(array, axis), dim)


def split_up(array, dim, count):
    lengths = array.shape
    blocks = array.reshape(*lengths[:dim], count, lengths[dim] // count, *lengths[dim + 1 :])
    return jnp.moveaxis(blocks, dim, 0)


def sum_at_owner(array, axis, dim):
    blocks = split_up(array, dim, lax.axis_size(axis))
    arrived = lax.all_to_all(blocks, axis, split_axis=0, concat_axis=0, tiled=True)
    return arrived.astype(jnp.float32).sum(axis=0)


def trailing_means(extended, row_count, lead_rows, first_position):
    group_width = extended.shape[1] // 4
    position = first_position + jnp.arange(row_count, dtype=jnp.int32)
    pieces = []
    for scale_index in range(4):
        window = 2 ** (scale_index + 1)
        channel_block = extended[:, scale_index * group_width : (scale_index + 1) * group_width]
        window_sum = channel_block[lead_rows : lead_rows + row_count]
        for back_step in range(1, window):
            window_sum = (
                window_sum
                + channel_block[lead_rows - back_step : lead_rows - back_step + row_count]
            )
        divisor = jnp.minimum(position + 1, window).astype(jnp.float32)
        pieces.append(window_sum / divisor[:, None])
    return jnp.concatenate(pieces, axis=1)


def route_terms(group_logits, inner_logits, group_pick, inner_pick, per_group):
    group_ids = jnp.arange(group_logits.shape[1], dtype=jnp.int32)
    chosen = jnp.sum(
        jnp.where(group_pick[:, None] == group_ids[None, :], group_logits, 0.0), axis=1
    )
    group_share = 1.0 / jnp.sum(jnp.exp(group_logits - chosen[:, None]), axis=1)
    target = group_pick[:, None] * per_group + inner_pick
    expert_ids = jnp.arange(inner_logits.shape[1], dtype=jnp.int32)
    picked = jnp.sum(
        jnp.where(target[:, :, None] == expert_ids[None, None, :], inner_logits[:, None, :], 0.0),
        axis=2,
    )
    first_share = jax.nn.sigmoid(picked[:, 0] - picked[:, 1])
    route_weight = group_share[:, None] * jnp.stack([first_share, 1.0 - first_share], axis=1)
    return (target, route_weight)


def slot_terms(target, expert_count, capacity):
    expert_ids = jnp.arange(expert_count, dtype=jnp.int32)
    expert_hits = (target[:, :, None] == expert_ids[None, None, :]).astype(jnp.int32)
    per_token = jnp.sum(expert_hits, axis=1)
    earlier = jnp.cumsum(per_token, axis=0) - per_token
    route_rank = jnp.sum(expert_hits * earlier[:, None, :], axis=2)
    is_kept = route_rank < capacity
    slot_index = target * capacity + jnp.minimum(route_rank, capacity - 1)
    return (slot_index, is_kept)


def slot_sources(slot_index, is_kept, slot_count):
    token_ids = jnp.broadcast_to(
        jnp.arange(slot_index.shape[0], dtype=jnp.int32)[:, None], slot_index.shape
    )
    placed = jnp.where(is_kept, slot_index, slot_count).reshape(-1)
    source = jnp.zeros((slot_count,), jnp.int32).at[placed].set(token_ids.reshape(-1), mode="drop")
    slot_used = jnp.zeros((slot_count,), jnp.bool_).at[placed].set(True, mode="drop")
    return (source, slot_used)


def per_device(
    mix_input,
    pool_weight,
    pool_scale,
    out_weight,
    moe_input,
    moe_gain,
    group_router,
    inner_router,
    group_pick,
    inner_pick,
    gate_weight,
    up_weight,
    down_weight,
):
    row_count = mix_input.shape[0]
    reach_back = WINDOW_MAX - 1
    before = passed_along(mix_input[row_count - reach_back :], ("ep", "tp"), 1)
    extended = jnp.concatenate([before, mix_input], axis=0).astype(jnp.float32)
    first_position = lax.axis_index(("ep", "tp")) * row_count
    trailing = (
        trailing_means(extended, row_count, reach_back, first_position) - extended[reach_back:]
    )
    pooled = trailing.astype(jnp.bfloat16)
    groups, group_dim = (pool_weight.shape[0], pool_weight.shape[1])
    grouped = jnp.einsum(
        "tgc,gcd->tgd",
        pooled.reshape(row_count, groups, group_dim),
        pool_weight,
        preferred_element_type=jnp.float32,
    )
    grouped = (grouped.reshape(row_count, groups * group_dim) * pool_scale[None, :]).astype(
        jnp.bfloat16
    )
    mix_out = jnp.dot(grouped, out_weight, preferred_element_type=jnp.float32).astype(jnp.bfloat16)
    tokens, feature_width = moe_input.shape
    token_values = moe_input.astype(jnp.float32)
    norm_scale = lax.rsqrt(
        jnp.maximum(jnp.mean(token_values * token_values, axis=1, keepdims=True), NORM_FLOOR)
    )
    normed = (token_values * norm_scale * moe_gain[None, :]).astype(jnp.bfloat16)
    group_logits = jnp.dot(normed, group_router, preferred_element_type=jnp.float32)
    inner_logits = jnp.dot(normed, inner_router, preferred_element_type=jnp.float32)
    group_count = group_router.shape[1]
    expert_count = inner_router.shape[1]
    target, route_weight = route_terms(
        group_logits, inner_logits, group_pick, inner_pick, expert_count // group_count
    )
    capacity = 2 * inner_pick.shape[1] * tokens // expert_count
    slot_index, is_kept = slot_terms(target, expert_count, capacity)
    source, slot_used = slot_sources(slot_index, is_kept, expert_count * capacity)
    tp_count = lax.axis_size("tp")
    slice_width = feature_width // tp_count
    gate_local = gate_weight[0]
    up_local = up_weight[0]
    own_columns = lax.dynamic_slice_in_dim(
        normed, lax.axis_index("tp") * slice_width, slice_width, 1
    )
    outgoing = jnp.where(slot_used[:, None], own_columns[source], jnp.zeros((), jnp.bfloat16))
    arrived = lax.all_to_all(outgoing, "ep", split_axis=0, concat_axis=0, tiled=True)
    column_piece = gather_directly(arrived, "tp", 1)
    gate_sum = jnp.dot(column_piece, gate_local, preferred_element_type=jnp.float32)
    up_sum = jnp.dot(column_piece, up_local, preferred_element_type=jnp.float32)
    hidden = (jax.nn.silu(gate_sum) * up_sum).astype(jnp.bfloat16)
    down_local = down_weight[0]
    expert_result = sum_at_owner(
        lax.dot_general(
            down_local, hidden, (((0,), (1,)), ((), ())), preferred_element_type=jnp.float32
        ).astype(jnp.bfloat16),
        "tp",
        0,
    ).astype(jnp.bfloat16)
    returned = lax.all_to_all(expert_result, "ep", split_axis=1, concat_axis=1, tiled=True)
    route_scale = jnp.where(is_kept, route_weight, 0.0).astype(jnp.bfloat16)
    route_scale = lax.optimization_barrier(route_scale).astype(jnp.float32)
    picked = jnp.take(returned, slot_index, axis=1).astype(jnp.float32)
    combined = jnp.sum(picked * route_scale[None, :, :], axis=2)
    moe_out = combined.T.astype(jnp.bfloat16)
    return (mix_out, moe_out)


def solution(mesh):
    in_specs = (
        P(("ep", "tp"), None),
        P(),
        P(),
        P(),
        P("ep", None),
        P(),
        P(),
        P(),
        P("ep"),
        P("ep", None),
        P("ep", None, "tp"),
        P("ep", None, "tp"),
        P("ep", "tp", None),
    )
    out_specs = (P(("ep", "tp"), None), P("ep", "tp"))
    return jax.shard_map(
        per_device, mesh=mesh, in_specs=in_specs, out_specs=out_specs, check_vma=False
    )
```

profile of v0, /device:TPU:1, one launch (start us, length us, event | category | flops | bytes accessed | tf_op | source)
XLA Modules:
  0.0 145.5 jit_solution(8999248698207571175)
XLA Ops:
  0.6 0.7 broadcast_multiply_fusion
  1.4 0.7 broadcast_add_fusion
  2.2 0.2 reduce_window_sum.11
  2.5 0.7 broadcast_select_fusion.1
  3.2 0.1 copy.46
  3.3 0.1 reshape.118
  3.5 0.1 reshape.150
  3.6 1.4 scatter_custom_fusion.1
  5.0 1.2 fusion.1
  6.3 1.5 %scatter_custom_fusion = pred[512]{0:T(512)(128)(4,1)S(1)} fusion(s32[256]{0:T(256)S(1)} %bitcast.52, pred[256]{0:T(512)(128)(4,1)S(1)} %broadcast.124, pred[]{:T(512)} %constant.36.clone.1), kind=kCustom, calls=%fused_computation.90 | custom fusion | bytes 513 | tf_op jit(solution)/shard_map/scatter | solution.py:99
  7.9 1.2 fusion.3
  9.1 0.8 copy-done.1
  9.9 2.0 %gather_fusion = bf16[512,512]{1,0:T(8,128)(2,1)S(1)} fusion(bf16[128,512]{1,0:T(8,128)(2,1)S(1)} %constant_dynamic-slice_fusion, s32[1024]{0:T(1024)S(1)} %pad_clamp_fusion.1), kind=kCustom, calls=%fused_computation | custom fusion | bytes 1050624 | tf_op jit(solution)/shard_map/gather | solution.py:161
  11.9 0.1 bitcast_select_fusion
  12.0 30.5 %all_to_all.28 = bf16[64,8,512]{2,1,0:T(8,128)(2,1)S(1)} all-to-all(bf16[64,8,512]{2,1,0:T(8,128)(2,1)S(1)} %bitcast_select_fusion), channel_id=1, replica_groups=mesh['ep'=64,'tp'=4] {'ep'}, dimensions={0} | all-to-all | bytes 1048576 | tf_op jit(solution)/shard_map/all_to_all | solution.py:162
  42.5 0.2 copy.47
  42.7 1.5 %broadcast_in_dim.102 = bf16[4,512,512]{1,2,0:T(8,128)(2,1)} broadcast(bf16[512,512]{0,1:T(8,128)(2,1)S(1)} %copy.47), dimensions={1,2} | broadcast | bytes 2621440 | tf_op jit(solution)/shard_map/broadcast_in_dim | solution.py:27
  44.2 4.3 %all-to-all-start.1 = ((bf16[4,512,512]{1,2,0:T(8,128)(2,1)}), bf16[4,512,512]{1,2,0:T(8,128)(2,1)S(1)}, u32[]{:S(2)}, u32[]{:S(2)}) async-start(bf16[4,512,512]{1,2,0:T(8,128)(2,1)} %broadcast_in_dim.102), calls=%async_computation.1 | async-start | bytes 4194304 | tf_op jit(solution)/shard_map/all_to_all | solution.py:26
  48.6 0.8 slice.136
  49.3 3.4 %collective-permute-start = (bf16[15,1024]{1,0:T(8,128)(2,1)S(1)}, bf16[15,1024]{1,0:T(8,128)(2,1)S(1)}, u32[]{:S(2)}, u32[]{:S(2)}) collective-permute-start(bf16[15,1024]{1,0:T(8,128)(2,1)S(1)} %slice.136), channel_id=1, source_target_pairs={{0,1},{1,2},{2,3},{3,4},{4,5},{5,6},{6,7},{7,8},{8,9},{9,10},{10,1... | collective-permute-start | bytes 92168 | tf_op jit(solution)/shard_map/ppermute | solution.py:15
  52.7 0.1 copy.49
  52.9 0.1 reshape.132
  53.0 1.3 select_reduce_fusion.2
  54.4 19.9 %all-to-all-done.1 = bf16[4,512,512]{1,2,0:T(8,128)(2,1)S(1)} async-done(((bf16[4,512,512]{1,2,0:T(8,128)(2,1)}), bf16[4,512,512]{1,2,0:T(8,128)(2,1)S(1)}, u32[]{:S(2)}, u32[]{:S(2)}) %all-to-all-start.1) | async-done | bytes 2097184 | tf_op jit(solution)/shard_map/all_to_all | solution.py:26
  74.3 2.8 %fusion.9 = f32[512,256]{1,0:T(8,128)} fusion(bf16[512,2048]{0,1:T(8,128)(2,1)S(1)} %bitcast.47, bf16[1,2048,256]{2,1,0:T(8,128)(2,1)} %param.23), kind=kOutput, calls=%fused_computation.20 | convolution fusion | flops 536870912 | bytes 3670016 | tf_op jit(solution)/shard_map/dot_general | solution.py:164
  77.1 5.0 %convolution_convert_fusion = bf16[512,2048]{1,0:T(8,128)(2,1)} fusion(bf16[512,2048]{0,1:T(8,128)(2,1)S(1)} %bitcast.48, bf16[1,256,2048]{2,1,0:T(8,128)(2,1)S(1)} %copy-done, bf16[1,2048,256]{2,1,0:T(8,128)(2,1)} %param.24, f32[512,256]{1,0:T(8,128)} %fusion.9), kind=kOutput, calls=%fused_computation.4 | convolution fusion | flops 1075576832 | bytes 6815744 | tf_op jit(solution)/shard_map/dot_general | solution.py:169
  82.1 3.1 %copy.59 = bf16[64,4,8,512]{3,2,0,1:T(8,128)(2,1)} copy(bf16[64,4,8,512]{3,2,1,0:T(8,128)(2,1)} %bitcast.49) | data formatting | bytes 4194304 | tf_op jit(solution)/shard_map/reshape | solution.py:37
  85.2 4.6 %all-to-all-start.2 = ((bf16[4,512,512]{1,2,0:T(8,128)(2,1)}), bf16[4,512,512]{1,2,0:T(8,128)(2,1)}, u32[]{:S(2)}, u32[]{:S(2)}) async-start(bf16[4,512,512]{1,2,0:T(8,128)(2,1)} %bitcast.45), calls=%async_computation.2 | async-start | bytes 4194304 | tf_op jit(solution)/shard_map/all_to_all | solution.py:43
  89.8 0.3 fusion.32
  90.2 0.6 minimum_convert_fusion.2
  90.8 0.1 copy.50
  90.9 0.7 copy.45
  91.6 0.1 maximum_convert_fusion
  91.8 1.0 fusion.23
  92.8 21.6 %all-to-all-done.2 = bf16[4,512,512]{1,2,0:T(8,128)(2,1)} async-done(((bf16[4,512,512]{1,2,0:T(8,128)(2,1)}), bf16[4,512,512]{1,2,0:T(8,128)(2,1)}, u32[]{:S(2)}, u32[]{:S(2)}) %all-to-all-start.2) | async-done | bytes 2097184 | tf_op jit(solution)/shard_map/all_to_all | solution.py:43
  114.4 2.9 %reduce_sum.78 = bf16[512,512]{0,1:T(8,128)(2,1)} reduce(bf16[4,512,512]{1,2,0:T(8,128)(2,1)} %all-to-all-done.2, bf16[]{:T(256)} %constant.70.clone.1), dimensions={0}, to_apply=%region_6.7 | reduce | flops 786432 | bytes 2621442 | tf_op jit(solution)/shard_map/reduce_sum | solution.py:44
  117.3 7.8 %all-to-all-start.3 = ((bf16[512,64,8]{0,2,1:T(8,128)(2,1)}), bf16[512,64,8]{0,2,1:T(8,128)(2,1)S(1)}, u32[]{:S(2)}, u32[]{:S(2)}) async-start(bf16[512,64,8]{0,2,1:T(8,128)(2,1)} %bitcast.12), calls=%async_computation.3 | async-start | bytes 1048576 | tf_op jit(solution)/shard_map/all_to_all | solution.py:175
  125.1 0.3 fusion.20
  125.4 0.6 copy-done.11
  126.0 0.4 fusion.11
  126.4 0.3 copy-done.8
  126.7 0.2 fusion.5
  126.9 1.3 copy-done.10
  128.2 2.3 %convolution_convert_fusion.1 = bf16[256,2048]{1,0:T(8,128)(2,1)} fusion(bf16[256,1024]{0,1:T(8,128)(2,1)S(1)} %fusion.5, bf16[1024,2048]{1,0:T(8,128)(2,1)S(1)} %copy-done.10), kind=kOutput, calls=%fused_computation.5 | convolution fusion | flops 1074266112 | bytes 5767168 | tf_op jit(solution)/shard_map/dot_general | solution.py:137
  130.5 12.3 %all-to-all-done.3 = bf16[512,64,8]{0,2,1:T(8,128)(2,1)S(1)} async-done(((bf16[512,64,8]{0,2,1:T(8,128)(2,1)}), bf16[512,64,8]{0,2,1:T(8,128)(2,1)S(1)}, u32[]{:S(2)}, u32[]{:S(2)}) %all-to-all-start.3) | async-done | bytes 524320 | tf_op jit(solution)/shard_map/all_to_all | solution.py:175
  142.7 1.2 gather_fusion.1
  143.9 0.1 reshape.135
  144.0 1.5 %multiply_reduce_fusion = bf16[128,512]{1,0:T(8,128)(2,1)} fusion(bf16[128,2,512]{2,1,0:T(2,128)(2,1)S(1)} %reshape.135, pred[128,2]{1,0:T(8,128)(4,1)S(1)} %copy-done.5, f32[128,2]{1,0:T(8,128)S(1)} %copy.50), kind=kLoop, calls=%fused_computation.27 | loop fusion | flops 458752 | bytes 394496 | tf_op jit(solution)/shard_map/reduce_sum | solution.py:179
  (42 shorter events, 0.5 us)
Async XLA Ops:
  0.6 76.5 %copy-start = (bf16[1,256,2048]{2,1,0:T(8,128)(2,1)S(1)}, bf16[1,256,2048]{2,1,0:T(8,128)(2,1)}, u32[]{:S(2)}) copy-start(bf16[1,256,2048]{2,1,0:T(8,128)(2,1)} %param.25) | copy-start | bytes 3145732
  9.1 0.8 copy-start.1
  44.2 8.5 %copy-start.7 = (s32[128,2]{0,1:T(2,128)S(1)}, s32[128,2]{0,1:T(2,128)}, u32[]{:S(2)}) copy-start(s32[128,2]{0,1:T(2,128)} %param.22) | copy-start | bytes 3076
  44.2 8.8 %copy-start.6 = (bf16[2048,4]{0,1:T(4,128)(2,1)S(1)}, bf16[2048,4]{0,1:T(4,128)(2,1)}, u32[]{:S(2)}) copy-start(bf16[2048,4]{0,1:T(4,128)(2,1)} %param.19) | copy-start | bytes 49156
  44.2 8.8 %copy-start.9 = (s32[128]{0:T(128)S(1)}, s32[128]{0:T(128)}, u32[]{:S(2)}) copy-start(s32[128]{0:T(128)} %param.21) | copy-start | bytes 1540
  44.2 30.1 %all-to-all-start.1 = ((bf16[4,512,512]{1,2,0:T(8,128)(2,1)}), bf16[4,512,512]{1,2,0:T(8,128)(2,1)S(1)}, u32[]{:S(2)}, u32[]{:S(2)}) async-start(bf16[4,512,512]{1,2,0:T(8,128)(2,1)} %broadcast_in_dim.102), calls=%async_computation.1 | async-start | bytes 4194304 | tf_op jit(solution)/shard_map/all_to_all | solution.py:26
  49.3 42.3 %collective-permute-start = (bf16[15,1024]{1,0:T(8,128)(2,1)S(1)}, bf16[15,1024]{1,0:T(8,128)(2,1)S(1)}, u32[]{:S(2)}, u32[]{:S(2)}) collective-permute-start(bf16[15,1024]{1,0:T(8,128)(2,1)S(1)} %slice.136), channel_id=1, source_target_pairs={{0,1},{1,2},{2,3},{3,4},{4,5},{5,6},{6,7},{7,8},{8,9},{9,10},{10,1... | collective-permute-start | bytes 92168 | tf_op jit(solution)/shard_map/ppermute | solution.py:15
  85.2 4.6 %copy-start.2 = (bf16[128,2048]{1,0:T(8,128)(2,1)S(1)}, bf16[128,2048]{1,0:T(8,128)(2,1)}, u32[]{:S(2)}) copy-start(bf16[128,2048]{1,0:T(8,128)(2,1)} %copy-done.1) | copy-start | bytes 1572868
  85.2 4.6 %copy-start.4 = (bf16[2048,64]{0,1:T(8,128)(2,1)S(1)}, bf16[2048,64]{0,1:T(8,128)(2,1)}, u32[]{:S(2)}) copy-start(bf16[2048,64]{0,1:T(8,128)(2,1)} %param.20) | copy-start | bytes 786436
  85.2 6.4 %copy-start.3 = (bf16[256,1024]{1,0:T(8,128)(2,1)S(1)}, bf16[256,1024]{1,0:T(8,128)(2,1)}, u32[]{:S(2)}) copy-start(bf16[256,1024]{1,0:T(8,128)(2,1)} %param.13) | copy-start | bytes 1572868
  85.2 29.2 %all-to-all-start.2 = ((bf16[4,512,512]{1,2,0:T(8,128)(2,1)}), bf16[4,512,512]{1,2,0:T(8,128)(2,1)}, u32[]{:S(2)}, u32[]{:S(2)}) async-start(bf16[4,512,512]{1,2,0:T(8,128)(2,1)} %bitcast.45), calls=%async_computation.2 | async-start | bytes 4194304 | tf_op jit(solution)/shard_map/all_to_all | solution.py:43
  117.3 25.5 %all-to-all-start.3 = ((bf16[512,64,8]{0,2,1:T(8,128)(2,1)}), bf16[512,64,8]{0,2,1:T(8,128)(2,1)S(1)}, u32[]{:S(2)}, u32[]{:S(2)}) async-start(bf16[512,64,8]{0,2,1:T(8,128)(2,1)} %bitcast.12), calls=%async_computation.3 | async-start | bytes 1048576 | tf_op jit(solution)/shard_map/all_to_all | solution.py:175
  125.1 1.0 copy-start.11
  126.0 0.7 copy-start.8
  126.0 2.2 %copy-start.10 = (bf16[1024,2048]{1,0:T(8,128)(2,1)S(1)}, bf16[1024,2048]{1,0:T(8,128)(2,1)}, u32[]{:S(2)}) copy-start(bf16[1024,2048]{1,0:T(8,128)(2,1)} %param.16) | copy-start | bytes 12582916
  142.7 1.3 copy-start.5
where the time goes:
time: 146 us
  waiting for transfers between devices  53.8 us (37%)
  blocking collectives  30.5 us (21%)
  starting transfers between devices  20 us (14%)
  local copies, waits for them, and re-layouts  16.5 us (11%)
  matrix products  12 us (8%)
  other arithmetic  11.7 us (8%)
    all_to_all x1, blocking collectives, per_device(): lax.all_to_all(outgoing, 'ep', split_axis=0, concat_axis=0, tiled=True)  30.5 us
    all_to_all x1, waiting for transfers between devices, sum_at_owner(): lax.all_to_all(blocks, axis, split_axis=0, concat_axis=0, tiled=True)  21.6 us
    all_to_all x1, waiting for transfers between devices, sent_to_all(): lax.all_to_all(jnp.broadcast_to(array[None], (count, *array.shape)), axis...  19.9 us
    all_to_all x1, waiting for transfers between devices, per_device(): lax.all_to_all(expert_result, 'ep', split_axis=1, concat_axis=1, tiled=True)  12.3 us
    all_to_all x1, starting transfers between devices, per_device(): lax.all_to_all(expert_result, 'ep', split_axis=1, concat_axis=1, tiled=True)  7.79 us
    dot_general x1, matrix products, per_device(): lax.dot_general(down_local, hidden, (((0,), (1,)), ((), ())), preferred_e...  5.04 us
    all_to_all x1, starting transfers between devices, sum_at_owner(): lax.all_to_all(blocks, axis, split_axis=0, concat_axis=0, tiled=True)  4.57 us
    all_to_all x1, starting transfers between devices, sent_to_all(): lax.all_to_all(jnp.broadcast_to(array[None], (count, *array.shape)), axis...  4.31 us
  transfers between devices with their start and end apart: 4, of which 3 were waited for; matrix products, arithmetic and copies ran while one was open for 13% of the time, Pallas kernels for 0%

commit v1 on v0

v1 whole, which is shorter than its diff:
```python
import functools

import jax
import jax.numpy as jnp
from jax import lax
from jax.experimental import pallas as pl
from jax.experimental.pallas import tpu as pltpu
from jax.sharding import PartitionSpec as P

MESH = pl.DeviceIdType.MESH
NORM_FLOOR = 0.25
WINDOW_MAX = 16
HALO = 16
CAP = 8
PLANE = 8
F32 = jnp.float32
BF16 = jnp.bfloat16

SKEW_FORWARD = 1
SKEW_EXPERT = 2
SKEW_OPPOSITE = 3
SKEW_OWNER = 4


def kernel(
    n_ep,
    n_tp,
    mix_hbm,
    pool_hbm,
    pscale_hbm,
    outw_hbm,
    moe_hbm,
    gain_hbm,
    group_router_hbm,
    inner_router_hbm,
    group_pick_hbm,
    inner_pick_hbm,
    gate_hbm,
    up_hbm,
    down_hbm,
    mix_out,
    moe_out,
    mix_in,
    halo,
    pool_w,
    pscale,
    out_w,
    grouped,
    moe_in,
    gain,
    group_router,
    inner_router,
    group_pick,
    inner_pick,
    gate_w,
    up_w,
    down_w,
    normed,
    outgoing,
    arrived,
    partial,
    opp_left,
    opp_right,
    own_left,
    own_right,
    result,
    returned,
    spread_t,
    load_sem,
    own_sem,
    halo_send,
    halo_recv,
    disp_send,
    disp_recv,
    ag_send,
    ag_recv,
    rs_send,
    rs_recv,
    ret_send,
    ret_recv,
):
    n_planes = n_ep // PLANE
    half = PLANE // 2
    e = lax.axis_index("ep")
    t = lax.axis_index("tp")
    right, left = lax.rem(t + 1, n_tp), lax.rem(t + n_tp - 1, n_tp)
    opposite = lax.rem(t + 2, n_tp)
    plane = lax.div(e, PLANE)
    seat = lax.rem(e, PLANE)
    linear = e * n_tp + t
    n_all = n_ep * n_tp
    after = lax.rem(linear + 1, n_all)
    before = lax.rem(linear + n_all - 1, n_all)

    barrier = pltpu.get_barrier_semaphore()

    @pl.loop(1, n_ep)
    def _(step):
        pl.semaphore_signal(
            barrier, inc=1, device_id=(lax.rem(e + step, n_ep), t), device_id_type=MESH
        )

    for other in (right, left, opposite):
        pl.semaphore_signal(barrier, inc=1, device_id=(e, other), device_id_type=MESH)
    pl.semaphore_signal(
        barrier,
        inc=1,
        device_id=(lax.div(before, n_tp), lax.rem(before, n_tp)),
        device_id_type=MESH,
    )

    loads = [
        (group_pick_hbm, group_pick),
        (inner_pick_hbm, inner_pick),
        (moe_hbm, moe_in),
        (gain_hbm, gain),
        (mix_hbm, mix_in),
        (pool_hbm, pool_w),
        (pscale_hbm, pscale),
        (gate_hbm, gate_w),
        (up_hbm, up_w),
        (down_hbm, down_w),
        (outw_hbm, out_w),
        (inner_router_hbm, inner_router),
        (group_router_hbm, group_router),
    ]
    loads = [
        pltpu.make_async_copy(source, target, load_sem.at[index])
        for index, (source, target) in enumerate(loads)
    ]
    for load in loads:
        load.start()
    for load in loads[:4]:
        load.wait()

    n_tok = moe_in.shape[0]
    n_slot = n_ep * CAP
    group_row = group_pick[...]
    first = group_row * (n_ep // 4) + inner_pick[0:1, :]
    second = group_row * (n_ep // 4) + inner_pick[1:2, :]
    expert_row = lax.broadcasted_iota(jnp.int32, (n_ep, n_tok), 0)
    hit = (expert_row == first) | (expert_row == second)
    earlier_than = lax.broadcasted_iota(jnp.int32, (n_tok, n_tok), 0) < lax.broadcasted_iota(
        jnp.int32, (n_tok, n_tok), 1
    )
    hit_count = jnp.where(hit, 1.0, 0.0).astype(BF16)
    rank = jnp.dot(hit_count, jnp.where(earlier_than, 1.0, 0.0).astype(BF16), preferred_element_type=F32)
    rank = jnp.where(hit, rank, -1.0)
    slot_row = lax.broadcasted_iota(jnp.int32, (n_slot, n_ep), 0)
    slot_expert = lax.broadcasted_iota(jnp.int32, (n_slot, n_ep), 1) * CAP
    to_slot = jnp.where((slot_row >= slot_expert) & (slot_row < slot_expert + CAP), 1.0, 0.0).astype(BF16)
    slot_rank = jnp.dot(to_slot, rank.astype(BF16), preferred_element_type=F32)
    want_rank = lax.rem(lax.broadcasted_iota(jnp.int32, (n_slot, n_tok), 0), CAP).astype(F32)
    spread = jnp.where(slot_rank == want_rank, 1.0, 0.0)

    values = moe_in[...].astype(F32)
    scale = lax.rsqrt(jnp.maximum(jnp.mean(values * values, axis=1, keepdims=True), NORM_FLOOR))
    normed[...] = (values * scale * gain[...]).astype(BF16)
    width = outgoing.shape[2]
    own_columns = normed[:, pl.ds(pl.multiple_of(t * width, width), width)]
    outgoing[...] = (
        jnp.dot(spread.astype(BF16), own_columns, preferred_element_type=F32)
        .reshape(n_ep, CAP, width)
        .astype(BF16)
    )

    pl.semaphore_wait(barrier, n_ep - 1 + 3 + 1)

    def plane_at(step):
        size = lax.div(step + 1, 2)
        return size * (2 * lax.rem(step, 2) - 1)

    def source_plane(step):
        return lax.rem(plane - plane_at(step) + n_planes, n_planes)

    def target_plane(step):
        return lax.rem(plane + plane_at(step) + n_planes, n_planes)

    own_copy = pltpu.make_async_copy(outgoing.at[e], arrived.at[t, e], own_sem.at[0])
    own_copy.start()

    def send_block(step, peer):
        pltpu.make_async_remote_copy(
            src_ref=outgoing.at[peer],
            dst_ref=arrived.at[t, e],
            send_sem=disp_send,
            recv_sem=disp_recv.at[step],
            device_id=(peer, t),
            device_id_type=MESH,
        ).start()

    @pl.loop(1, PLANE)
    def _(turn):
        send_block(0, plane * PLANE + lax.rem(seat + turn, PLANE))

    @pl.loop(1, n_planes)
    def _(step):
        @pl.loop(0, PLANE)
        def _(turn):
            send_block(step, target_plane(step) * PLANE + lax.rem(seat + turn, PLANE))

    halo_copy = pltpu.make_async_remote_copy(
        src_ref=mix_hbm.at[pl.ds(mix_hbm.shape[0] - HALO, HALO)],
        dst_ref=halo,
        send_sem=halo_send,
        recv_sem=halo_recv,
        device_id=(lax.div(after, n_tp), lax.rem(after, n_tp)),
        device_id_type=MESH,
    )
    halo_copy.start()

    def to_neighbour(ref, target, send_sem, recv_sem, side):
        return pltpu.make_async_remote_copy(
            src_ref=ref,
            dst_ref=target,
            send_sem=send_sem,
            recv_sem=recv_sem,
            device_id=(e, side),
            device_id_type=MESH,
        )

    def drain(ref, sem):
        pltpu.make_async_copy(ref, ref, sem).wait()

    def rows_of(step):
        return source_plane(step) * PLANE

    def share(step):
        base = rows_of(step)
        block = arrived.at[t, pl.ds(base, PLANE)]

        @pl.when(step == 0)
        def _():
            own_copy.wait()
            drain(arrived.at[t, pl.ds(base, PLANE - 1)], disp_recv.at[step])

        @pl.when(step > 0)
        def _():
            drain(block, disp_recv.at[step])

        to_neighbour(block, block, ag_send.at[0], ag_recv.at[0, step], right).start()
        to_neighbour(block, block, ag_send.at[1], ag_recv.at[1, step], left).start()

    def forward(step):
        base = rows_of(step)
        drain(arrived.at[left, pl.ds(base, PLANE)], ag_recv.at[0, step])
        block = arrived.at[left, pl.ds(base, half)]
        to_neighbour(block, block, ag_send.at[2], ag_recv.at[2, step], right).start()
        drain(arrived.at[right, pl.ds(base, PLANE)], ag_recv.at[1, step])
        block = arrived.at[right, pl.ds(base + half, half)]
        to_neighbour(block, block, ag_send.at[3], ag_recv.at[3, step], left).start()

    def run_expert(step):
        base = rows_of(step)
        drain(arrived.at[opposite, pl.ds(base, half)], ag_recv.at[2, step])
        drain(arrived.at[opposite, pl.ds(base, half)], ag_recv.at[3, step])
        gate_sum, up_sum = 0.0, 0.0
        for piece in range(n_tp):
            rows = arrived[piece, pl.ds(base, PLANE)].reshape(PLANE * CAP, width)
            part = pl.ds(piece * width, width)
            gate_sum += jnp.dot(rows, gate_w[part, :], preferred_element_type=F32)
            up_sum += jnp.dot(rows, up_w[part, :], preferred_element_type=F32)
        hidden = (gate_sum / (1.0 + jnp.exp(-gate_sum)) * up_sum).astype(BF16)
        for piece in range(n_tp):
            product = jnp.dot(
                hidden, down_w[:, piece * width : (piece + 1) * width], preferred_element_type=F32
            )
            partial[piece, pl.ds(base, PLANE)] = product.reshape(PLANE, CAP, width).astype(BF16)
        to_neighbour(
            partial.at[opposite, pl.ds(base, half)],
            opp_left.at[step],
            rs_send.at[0],
            rs_recv.at[0, step],
            right,
        ).start()
        to_neighbour(
            partial.at[opposite, pl.ds(base + half, half)],
            opp_right.at[step],
            rs_send.at[1],
            rs_recv.at[1, step],
            left,
        ).start()

    def add_opposite(step):
        base = rows_of(step)
        for lane, (slot, start, side, target) in enumerate(
            (
                (opp_left, base, right, own_left),
                (opp_right, base + half, left, own_right),
            )
        ):
            drain(slot.at[step], rs_recv.at[lane, step])
            rows = pl.ds(start, half)
            partial[side, rows] = (partial[side, rows].astype(F32) + slot[step].astype(F32)).astype(BF16)
            to_neighbour(
                partial.at[side, pl.ds(base, PLANE)],
                target.at[step],
                rs_send.at[2 + lane],
                rs_recv.at[2 + lane, step],
                side,
            ).start()

    def finish(step):
        base = rows_of(step)
        drain(own_left.at[step], rs_recv.at[2, step])
        drain(own_right.at[step], rs_recv.at[3, step])
        rows = pl.ds(base, PLANE)
        result[rows] = (
            partial[t, rows].astype(F32) + own_left[step].astype(F32) + own_right[step].astype(F32)
        ).astype(BF16)

        def give_back(turn):
            peer = base + lax.rem(seat + turn, PLANE)
            pltpu.make_async_remote_copy(
                src_ref=result.at[peer],
                dst_ref=returned.at[e],
                send_sem=ret_send,
                recv_sem=ret_recv.at[step],
                device_id=(peer, t),
                device_id_type=MESH,
            ).start()

        @pl.when(step == 0)
        def _():
            pltpu.make_async_copy(result.at[e], returned.at[e], own_sem.at[1]).start()

            @pl.loop(1, PLANE)
            def _(turn):
                give_back(turn)

        @pl.when(step > 0)
        def _():
            @pl.loop(0, PLANE)
            def _(turn):
                give_back(turn)

    rows_mix = mix_in.shape[0]

    def pool():
        halo_copy.wait()
        for load in loads[4:7]:
            load.wait()
        lead = jnp.where(linear > 0, halo[...].astype(F32), 0.0)
        position = linear * rows_mix + lax.broadcasted_iota(jnp.int32, (rows_mix, 1), 0)
        scale_width = mix_in.shape[1] // 4
        pool_dim = pool_w.shape[1]
        for index in range(4):
            columns = slice(index * scale_width, (index + 1) * scale_width)
            own = mix_in[:, columns].astype(F32)
            total = jnp.concatenate([lead[:, columns], own], axis=0)
            for doubling in range(index + 1):
                total = total + pltpu.roll(total, 2**doubling, 0)
            divisor = jnp.minimum(position + 1, 2 ** (index + 1)).astype(F32)
            pooled = (total[HALO:] / divisor - own).astype(BF16)
            for part in range(scale_width // pool_dim):
                group = index * (scale_width // pool_dim) + part
                product = jnp.dot(
                    pooled[:, part * pool_dim : (part + 1) * pool_dim],
                    pool_w[group],
                    preferred_element_type=F32,
                )
                span = slice(group * pool_dim, (group + 1) * pool_dim)
                grouped[:, span] = (product * pscale[:, span]).astype(BF16)
        loads[10].wait()

    def project(piece):
        columns = pl.ds(pl.multiple_of(piece * width, width), width)
        mix_out[:, columns] = jnp.dot(
            grouped[...], out_w[:, columns], preferred_element_type=F32
        ).astype(BF16)

    pool()
    for load in loads[7:10]:
        load.wait()

    @pl.loop(0, n_planes + SKEW_OWNER)
    def _(now):
        def at(skew, stage):
            @pl.when((now >= skew) & (now < n_planes + skew))
            def _():
                stage(now - skew)

        at(0, share)
        at(SKEW_FORWARD, forward)
        at(SKEW_EXPERT, run_expert)
        at(SKEW_OPPOSITE, add_opposite)
        at(SKEW_OWNER, finish)

        @pl.when(now < 4)
        def _():
            project(now)

    for load in loads[11:]:
        load.wait()
    contract_last = (((1,), (1,)), ((), ()))
    group_logits = lax.dot_general(
        group_router[...], normed[...], contract_last, preferred_element_type=F32
    )
    inner_logits = lax.dot_general(
        inner_router[...], normed[...], contract_last, preferred_element_type=F32
    )
    group_ids = lax.broadcasted_iota(jnp.int32, group_logits.shape, 0)
    chosen = jnp.sum(jnp.where(group_ids == group_row, group_logits, 0.0), axis=0, keepdims=True)
    group_share = 1.0 / jnp.sum(jnp.exp(group_logits - chosen), axis=0, keepdims=True)
    picked_first = jnp.sum(jnp.where(expert_row == first, inner_logits, 0.0), axis=0, keepdims=True)
    picked_second = jnp.sum(jnp.where(expert_row == second, inner_logits, 0.0), axis=0, keepdims=True)
    first_share = jax.nn.sigmoid(picked_first - picked_second)
    route_weight = jnp.where(
        expert_row == first,
        group_share * first_share,
        jnp.where(expert_row == second, group_share * (1.0 - first_share), 0.0),
    )
    slot_weight = jnp.dot(to_slot, route_weight.astype(BF16), preferred_element_type=F32)
    spread_t[...] = jnp.transpose(spread * slot_weight).astype(BF16)

    pltpu.make_async_copy(result.at[e], returned.at[e], own_sem.at[1]).wait()
    drain(returned.at[pl.ds(0, PLANE - 1)], ret_recv.at[0])

    @pl.loop(1, n_planes)
    def _(step):
        drain(returned.at[pl.ds(0, PLANE)], ret_recv.at[step])

    moe_out[...] = jnp.dot(
        spread_t[...], returned[...].reshape(n_slot, width), preferred_element_type=F32
    ).astype(BF16)

    drain(outgoing.at[pl.ds(0, n_ep - 1)], disp_send)
    drain(result.at[pl.ds(0, n_ep - 1)], ret_send)
    for lane, ref in enumerate((returned, returned, opp_left, opp_right)):
        drain(ref, ag_send.at[lane])
    for lane, ref in enumerate((opp_left, opp_right, own_left, own_right)):
        drain(ref, rs_send.at[lane])


def per_device(
    n_ep,
    n_tp,
    mix_input,
    pool_weight,
    pool_scale,
    out_weight,
    moe_input,
    moe_gain,
    group_router,
    inner_router,
    group_pick,
    inner_pick,
    gate_weight,
    up_weight,
    down_weight,
):
    rows, channels = mix_input.shape
    tokens, features = moe_input.shape
    width = features // n_tp
    hidden = gate_weight.shape[2]
    n_planes = n_ep // PLANE
    half = PLANE // 2
    operands = (
        mix_input,
        pool_weight,
        pool_scale.reshape(1, -1),
        out_weight,
        moe_input,
        moe_gain.reshape(1, -1),
        group_router.T,
        inner_router.T,
        group_pick.reshape(1, -1),
        inner_pick.T,
        gate_weight[0],
        up_weight[0],
        down_weight[0],
    )

    def like(array):
        return pltpu.VMEM(array.shape, array.dtype)

    (mix, pool, pscale, outw, moe, gain, grouter, irouter, gpick, ipick, gate, up, down) = operands
    slots = pltpu.VMEM((n_ep, CAP, width), BF16)
    by_step = pltpu.VMEM((n_planes, PLANE, CAP, width), BF16)
    half_step = pltpu.VMEM((n_planes, half, CAP, width), BF16)
    dma = pltpu.SemaphoreType.DMA
    return pl.pallas_call(
        functools.partial(kernel, n_ep, n_tp),
        out_shape=(
            jax.ShapeDtypeStruct((rows, outw.shape[1]), BF16),
            jax.ShapeDtypeStruct((tokens, width), BF16),
        ),
        in_specs=[pl.BlockSpec(memory_space=pl.ANY)] * len(operands),
        out_specs=(pl.BlockSpec(memory_space=pltpu.VMEM), pl.BlockSpec(memory_space=pltpu.VMEM)),
        scratch_shapes=[
            like(mix),
            pltpu.VMEM((HALO, channels), BF16),
            like(pool),
            like(pscale),
            like(outw),
            pltpu.VMEM((rows, channels), BF16),
            like(moe),
            like(gain),
            like(grouter),
            like(irouter),
            like(gpick),
            like(ipick),
            like(gate),
            like(up),
            like(down),
            pltpu.VMEM((tokens, features), BF16),
            slots,
            pltpu.VMEM((n_tp, n_ep, CAP, width), BF16),
            pltpu.VMEM((n_tp, n_ep, CAP, width), BF16),
            half_step,
            half_step,
            by_step,
            by_step,
            slots,
            slots,
            pltpu.VMEM((tokens, n_ep * CAP), BF16),
            dma((len(operands),)),
            dma((2,)),
            dma,
            dma,
            dma,
            dma((n_planes,)),
            dma((4,)),
            dma((4, n_planes)),
            dma((4,)),
            dma((4, n_planes)),
            dma,
            dma((n_planes,)),
        ],
        compiler_params=pltpu.CompilerParams(collective_id=0, has_side_effects=True),
    )(*operands)


def solution(mesh):
    in_specs = (
        P(("ep", "tp"), None),
        P(),
        P(),
        P(),
        P("ep", None),
        P(),
        P(),
        P(),
        P("ep"),
        P("ep", None),
        P("ep", None, "tp"),
        P("ep", None, "tp"),
        P("ep", "tp", None),
    )
    out_specs = (P(("ep", "tp"), None), P("ep", "tp"))
    return jax.shard_map(
        functools.partial(per_device, mesh.shape["ep"], mesh.shape["tp"]),
        mesh=mesh,
        in_specs=in_specs,
        out_specs=out_specs,
        check_vma=False,
    )
```

time: 146 us -> 77.5 us (0.53)
  Pallas kernels: 0 us -> 71.8 us
  waiting for transfers between devices: 53.8 us -> 0 us
  blocking collectives: 30.5 us -> 0 us
  starting transfers between devices: 20 us -> 0 us
  local copies, waits for them, and re-layouts: 16.5 us -> 3.87 us
  matrix products: 12 us -> 0 us
  other arithmetic: 11.7 us -> 0 us
    pallas_call x0 -> x1, Pallas kernels: none -> 71.8 us  [per_device(): pl.pallas_call(functools.partial(kernel, n_ep, n_tp), out_shape=(jax.Shap...]
    all_to_all x3 -> x0, waiting for transfers between devices: 53.8 us -> none  [the longest x1 21.6 us: sum_at_owner(): lax.all_to_all(blocks, axis, split_axis=0, concat_axis=0, tiled=True)]
    all_to_all x1 -> x0, blocking collectives: 30.5 us -> none  [per_device(): lax.all_to_all(outgoing, 'ep', split_axis=0, concat_axis=0, tiled=True)]
    all_to_all x3 -> x0, starting transfers between devices: 16.7 us -> none  [the longest x1 7.79 us: per_device(): lax.all_to_all(expert_result, 'ep', split_axis=1, concat_axis=1, tiled=True)]
    dot_general x6 -> x0, matrix products: 12 us -> none  [the longest x1 5.04 us: per_device(): lax.dot_general(down_local, hidden, (((0,), (1,)), ((), ())), preferred_e...]
    reduce_sum x7 -> x0, other arithmetic: 5.72 us -> none  [the longest x1 2.86 us: sum_at_owner(): return arrived.astype(jnp.float32).sum(axis=0)]
    ppermute x1 -> x0, starting transfers between devices: 3.37 us -> none  [passed_along(): lax.ppermute(value, axis, [(source, source + steps) for source in range(f...]
    reshape x3 -> x0, local copies, waits for them, and re-layouts: 3.36 us -> none  [the longest x1 3.08 us: split_up(): array.reshape(*lengths[:dim], count, lengths[dim] // count, *lengths[dim...]
  transfers between devices with their start and end apart: 4 -> 0, of which waited for: 3 -> 0; matrix products, arithmetic and copies ran while one was open for 13% -> 0% of each run, Pallas kernels for 0% -> 0%
where the time goes in v1:
time: 77.5 us; the launch traced here: 76.3 us
  Pallas kernels  71.8 us (93%)
  local copies, waits for them, and re-layouts  3.87 us (5%)
    pallas_call x1, Pallas kernels, per_device(): pl.pallas_call(functools.partial(kernel, n_ep, n_tp), out_shape=(jax.Shap...  71.8 us
    unnamed x2, local copies, waits for them, and re-layouts  3.87 us

profile of v1, /device:TPU:1, one launch (start us, length us, event | category | flops | bytes accessed | tf_op | source)
XLA Modules:
  0.0 76.3 jit_solution(3777713045277446525)
XLA Ops:
  0.6 71.8 %shard_map.140 = (bf16[256,2048]{1,0:T(8,128)(2,1)}, bf16[128,512]{1,0:T(8,128)(2,1)}) custom-call(bf16[256,1024]{1,0:T(8,128)(2,1)} %mix_hbm.1, bf16[8,128,128]{2,1,0:T(8,128)(2,1)} %pool_hbm.1, f32[1,1024]{1,0:T(1,128)} %bitcast.15, bf16[1024,2048]{1,0:T(8,128)(2,1)} %outw_hbm.1, bf16[128,2048]{1,0:T(8,128)(2,1)} %moe_hbm.1, f32[1,2048]{1,0:T(1,128)} %bitcast.14, ...), custom_call_target="tpu_custom_call" | custom-call | tf_op jit(solution)/shard_map/pallas_call | solution.py:482
  72.4 2.3 %copy.17 = bf16[256,2048]{1,0:T(8,128)(2,1)} copy(bf16[256,2048]{1,0:T(8,128)(2,1)} %get-tuple-element.4) | data formatting | bytes 2097152
  74.7 1.6 %copy.18 = bf16[128,512]{1,0:T(8,128)(2,1)} copy(bf16[128,512]{1,0:T(8,128)(2,1)} %get-tuple-element.5) | data formatting | bytes 262144
